TPU v7x, 32 devices: a whole 2x2x4 slice. The times are simulated.
32 devices in a mesh: fs: 4 (over z), rep: 4 (over y, x), tp: 2 (over core).
Axes of the slice: x: 2, y: 2, z: 4, core: 2. Of those that a mesh axis runs over, the one named last changes fastest.
Arguments:
- mixer_input: bfloat16 [32768, 2048], P(('fs', 'rep')), may hold values from -6 to 6
- value_cot: bfloat16 [32768, 2048], P(('fs', 'rep'), 'tp'), may hold values from -0.22097087 to 0.22097087
- gate_cot: bfloat16 [32768, 2048], P(('fs', 'rep'), 'tp'), may hold values from -0.22097087 to 0.22097087
- value_weight: float32 [2048, 2048], P('fs', 'tp'), may hold values from -0.125 to 0.125
- gate_weight: float32 [2048, 2048], P('fs', 'tp'), may hold values from -0.125 to 0.125
- value_basis: bfloat16 [2048, 256], replicated, may hold values from -0.8838835 to 0.8838835
- gate_basis: bfloat16 [2048, 256], replicated, may hold values from -0.8838835 to 0.8838835
- value_first: float32 [256, 2048], P('fs', 'tp'), may hold values from -6 to 6
- gate_first: float32 [256, 2048], P('fs', 'tp'), may hold values from -6 to 6
- value_second: float32 [256, 2048], P('fs', 'tp'), may hold values from 0.01 to 1
- gate_second: float32 [256, 2048], P('fs', 'tp'), may hold values from 0.01 to 1
Outputs:
- value_new: float32 [2048, 2048], P('fs', 'tp')
- gate_new: float32 [2048, 2048], P('fs', 'tp')
- value_copy: bfloat16 [2048, 2048], P(None, 'tp')
- gate_copy: bfloat16 [2048, 2048], P(None, 'tp')
- value_step: float32 [2048, 2048], P('fs', 'tp')
- gate_step: float32 [2048, 2048], P('fs', 'tp')
- value_first_new: float32 [256, 2048], P('fs', 'tp')
- gate_first_new: float32 [256, 2048], P('fs', 'tp')
- value_second_new: float32 [256, 2048], P('fs', 'tp')
- gate_second_new: float32 [256, 2048], P('fs', 'tp')
All inputs are finite; a program needn't handle non-finite values.
Results may differ from a plain program's by a relative error of at most 0.0044.
Values may be sent and summed in bfloat16 or wider, within the bound.
A program may use at most 128 MiB of HBM per device.

v0:
```python
import jax
import jax.numpy as jnp
from jax import lax
from jax.sharding import PartitionSpec as P

D = 2048
learn_rate = 0.02


def local(
    mixer_input,
    value_cot,
    gate_cot,
    value_weight,
    gate_weight,
    value_basis,
    gate_basis,
    value_first,
    gate_first,
    value_second,
    gate_second,
):
    half_cols = value_cot.shape[1]
    rows_dev = value_weight.shape[0]
    fs_index = lax.axis_index("fs")
    own_value = lax.dynamic_slice_in_dim(value_basis, fs_index * rows_dev, rows_dev, 0)
    own_gate = lax.dynamic_slice_in_dim(gate_basis, fs_index * rows_dev, rows_dev, 0)
    value_proj = jnp.dot(mixer_input, value_basis, preferred_element_type=jnp.float32)
    gate_proj = jnp.dot(mixer_input, gate_basis, preferred_element_type=jnp.float32)
    upper_value = lax.optimization_barrier(value_proj.astype(jnp.bfloat16))
    upper_gate = lax.optimization_barrier(gate_proj.astype(jnp.bfloat16))
    lower_value = (value_proj - upper_value.astype(jnp.float32)).astype(jnp.bfloat16)
    lower_gate = (gate_proj - upper_gate.astype(jnp.float32)).astype(jnp.bfloat16)
    value_part = jnp.dot(upper_value.T, value_cot, preferred_element_type=jnp.float32) + jnp.dot(
        lower_value.T, value_cot, preferred_element_type=jnp.float32
    )
    gate_part = jnp.dot(upper_gate.T, gate_cot, preferred_element_type=jnp.float32) + jnp.dot(
        lower_gate.T, gate_cot, preferred_element_type=jnp.float32
    )
    partial_value = lax.psum_scatter(
        jnp.concatenate([value_part, gate_part], axis=1), "fs", scatter_dimension=0, tiled=True
    )
    projected = lax.psum(partial_value, "rep")
    value_small = projected[:, :half_cols]
    gate_small = projected[:, half_cols:]
    value_first_new = 0.9 * value_first + 0.1 * value_small
    gate_first_new = 0.9 * gate_first + 0.1 * gate_small
    value_second_new = 0.95 * value_second + 0.05 * value_small * value_small
    gate_second_new = 0.95 * gate_second + 0.05 * gate_small * gate_small
    scaled = jnp.concatenate(
        [
            value_first_new * lax.rsqrt(value_second_new),
            gate_first_new * lax.rsqrt(gate_second_new),
        ],
        axis=1,
    ).astype(jnp.bfloat16)
    piece = lax.all_gather(scaled, "fs", axis=0, tiled=True)
    value_part = jnp.dot(own_value, piece[:, :half_cols], preferred_element_type=jnp.float32)
    gate_part = jnp.dot(own_gate, piece[:, half_cols:], preferred_element_type=jnp.float32)
    expanded = jnp.concatenate([value_part, gate_part], axis=1)
    value_full = expanded[:, :half_cols]
    gate_full = expanded[:, half_cols:]
    squares = lax.psum(
        (jnp.sum(value_full * value_full), jnp.sum(gate_full * gate_full)), ("fs", "tp")
    )
    entries = float(D * D)
    value_step = value_full * lax.rsqrt(squares[0] / entries + 1e-06)
    gate_step = gate_full * lax.rsqrt(squares[1] / entries + 1e-06)
    value_new = value_weight - learn_rate * value_step
    gate_new = gate_weight - learn_rate * gate_step
    copies = (
        lax.all_gather(value_new.astype(jnp.bfloat16), "fs", axis=0, tiled=True),
        lax.all_gather(gate_new.astype(jnp.bfloat16), "fs", axis=0, tiled=True),
    )
    return (
        value_new,
        gate_new,
        copies[0],
        copies[1],
        value_step,
        gate_step,
        value_first_new,
        gate_first_new,
        value_second_new,
        gate_second_new,
    )


def solution(mesh):
    return jax.shard_map(
        local,
        mesh=mesh,
        in_specs=(
            P(("fs", "rep"), None),
            P(("fs", "rep"), "tp"),
            P(("fs", "rep"), "tp"),
            P("fs", "tp"),
            P("fs", "tp"),
            P(),
            P(),
            P("fs", "tp"),
            P("fs", "tp"),
            P("fs", "tp"),
            P("fs", "tp"),
        ),
        out_specs=(
            P("fs", "tp"),
            P("fs", "tp"),
            P(None, "tp"),
            P(None, "tp"),
            P("fs", "tp"),
            P("fs", "tp"),
            P("fs", "tp"),
            P("fs", "tp"),
            P("fs", "tp"),
            P("fs", "tp"),
        ),
        check_vma=False,
    )
```

profile of v0, /device:TPU:0, one launch (start us, length us, event | category | flops | bytes accessed | tf_op | source)
XLA Modules:
  0.0 350.1 jit_solution(15234940572082400259)
XLA Ops:
  7.2 0.0 copy-start
  7.2 0.0 reduce-scatter.2.cloned.1.call-start
  7.2 0.0 copy-start.9
  7.2 6.2 %fusion.15 = (bf16[2048,256]{1,0:T(8,128)(2,1)S(1)}, f32[2048,256]{1,0:T(8,128)S(1)}) fusion(bf16[2048,2048]{1,0:T(8,128)(2,1)} %param.11, bf16[2048,256]{1,0:T(8,128)(2,1)} %param.16), kind=kOutput, calls=%fused_computation.31 | convolution fusion | flops 2148007936 | bytes 12582912 | tf_op jit(solution)/shard_map/dot_general | solution.py:28
  13.5 0.0 copy-done
  13.5 0.1 copy-done.9
  13.6 2.4 fusion.14
  16.0 0.0 copy-done.1
  16.1 1.3 fusion.16
  17.3 0.0 copy-start.2
  17.3 1.3 convolution_add_fusion.1
  18.6 0.9 copy-done.2
  19.5 1.3 fusion.17
  20.8 1.3 convolution_add_fusion
  22.1 1.5 pad_maximum_fusion
  23.5 0.0 copy-start.5
  23.5 0.0 copy-start.6
  23.6 0.0 copy-start.8
  23.6 0.0 reduce-scatter.2.cloned.1.call-update
  23.6 0.0 all-reduce.3.cloned.1.call-start
  23.6 46.5 %reduce-scatter.2.cloned.1.call-done = f32[64,2048]{1,0:T(8,128)} async-done(((f32[256,2048]{1,0:T(8,128)}), f32[64,2048]{1,0:T(8,128)}) %reduce-scatter.2.cloned.1.call-update) | async-done | bytes 524304 | tf_op jit(solution)/shard_map/reduce_scatter | solution.py:40
  70.1 0.0 all-reduce.3.cloned.1.call-update
  70.1 0.0 all-gather.4.cloned.1.call-start
  70.2 47.5 %all-reduce.3.cloned.1.call-done = f32[64,2048]{1,0:T(8,128)} async-done(((f32[64,2048]{1,0:T(8,128)}), f32[64,2048]{1,0:T(8,128)}) %all-reduce.3.cloned.1.call-update) | async-done | bytes 524304 | tf_op jit(solution)/shard_map/psum | solution.py:43
  117.7 0.0 copy-done.5
  117.7 0.0 copy-done.6
  117.7 0.0 copy-done.7
  117.7 0.0 copy-done.8
  117.7 2.1 multiply_convert_fusion.1
  119.8 0.7 pad_maximum_fusion.1
  120.5 0.0 all-gather.4.cloned.1.call-update
  120.5 0.0 all-gather.6.cloned.1.call-start
  120.6 28.1 %all-gather.4.cloned.1.call-done = bf16[256,2048]{1,0:T(8,128)(2,1)} async-done(((bf16[64,2048]{1,0:T(8,128)(2,1)}), bf16[256,2048]{1,0:T(8,128)(2,1)}) %all-gather.4.cloned.1.call-update) | async-done | bytes 1048592 | tf_op jit(solution)/shard_map/all_gather | solution.py:57
  148.7 0.0 copy-start.4
  148.7 2.4 multiply_reduce_fusion
  151.1 0.0 copy-done.4
  151.1 3.5 multiply_reduce_fusion.1
  154.6 15.3 %all-reduce = (f32[]{:T(128)}, f32[]{:T(128)}) all-reduce(f32[]{:T(128)} %get-tuple-element.31, f32[]{:T(128)} %get-tuple-element.33), channel_id=1, replica_groups=mesh['fs'=4,'rep'=4,'tp'=2] {'fs','tp'}, use_global_device_ids=true, to_apply=%region_3.0 | all-reduce | flops 2 | bytes 16 | tf_op jit(solution)/shard_map/psum | solution.py:63
  170.6 5.6 %fusion.11 = (bf16[512,1024]{1,0:T(8,128)(2,1)}, f32[512,1024]{1,0:T(8,128)}, f32[512,1024]{1,0:T(8,128)}) fusion(f32[512,1024]{1,0:T(8,128)} %param.14, f32[512,1024]{1,0:T(8,128)} %get-tuple-element.32, f32[]{:T(128)S(6)} %rsqrt.14), kind=kLoop, calls=%fused_computation.29 | loop fusion | flops 2097152 | bytes 9437188 | tf_op jit(solution)/shard_map/convert_element_type | solution.py:72
  176.2 0.0 all-gather.6.cloned.1.call-update
  176.2 0.0 all-gather.8.cloned.1.call-start
  177.0 4.8 %fusion.10 = (bf16[512,1024]{1,0:T(8,128)(2,1)}, f32[512,1024]{1,0:T(8,128)}, f32[512,1024]{1,0:T(8,128)}) fusion(f32[512,1024]{1,0:T(8,128)} %param.15, f32[512,1024]{1,0:T(8,128)S(1)} %get-tuple-element.34, f32[]{:T(128)S(6)} %rsqrt.15), kind=kLoop, calls=%fused_computation.28 | loop fusion | flops 2097152 | bytes 9437188 | tf_op jit(solution)/shard_map/convert_element_type | solution.py:73
  181.7 0.0 all-gather.8.cloned.1.call-update
  181.7 73.7 %all-gather.6.cloned.1.call-done = bf16[2048,1024]{1,0:T(8,128)(2,1)} async-done(((bf16[512,1024]{1,0:T(8,128)(2,1)}), bf16[2048,1024]{1,0:T(8,128)(2,1)}) %all-gather.6.cloned.1.call-update) | async-done | bytes 4194320 | tf_op jit(solution)/shard_map/all_gather | solution.py:72
  255.5 81.2 %all-gather.8.cloned.1.call-done = bf16[2048,1024]{1,0:T(8,128)(2,1)} async-done(((bf16[512,1024]{1,0:T(8,128)(2,1)}), bf16[2048,1024]{1,0:T(8,128)(2,1)}) %all-gather.8.cloned.1.call-update) | async-done | bytes 4194320 | tf_op jit(solution)/shard_map/all_gather | solution.py:73
  336.7 4.8 %copy.24 = bf16[2048,1024]{1,0:T(8,128)(2,1)} copy(bf16[2048,1024]{1,0:T(8,128)(2,1)} %all-gather.6.cloned.1.call-done) | data formatting | bytes 8388608
  341.5 0.0 copy-done.3
  341.5 2.0 copy.25
  (3 shorter events, 0.0 us)
Async XLA Ops:
  7.2 6.3 %copy-start = (bf16[2048,256]{1,0:T(8,128)(2,1)S(1)}, bf16[2048,256]{1,0:T(8,128)(2,1)}, u32[]{:S(2)}) copy-start(bf16[2048,256]{1,0:T(8,128)(2,1)} %param.17) | copy-start | bytes 3145732
  7.2 62.9 %reduce-scatter.2.cloned.1.call-start = ((), (), s32[]{:S(2)}) async-start(), calls=%async_computation.1 | async-start | bytes 2621440 | tf_op jit(solution)/shard_map/reduce_scatter | solution.py:40
  7.2 6.4 %copy-start.9 = (bf16[2048,2048]{1,0:T(8,128)(2,1)S(1)}, bf16[2048,2048]{1,0:T(8,128)(2,1)}, u32[]{:S(2)}) copy-start(bf16[2048,2048]{1,0:T(8,128)(2,1)} %param.11) | copy-start | bytes 25165828
  13.6 2.4 copy-start.1
  17.3 2.2 copy-start.2
  23.5 94.1 %copy-start.5 = (f32[64,1024]{1,0:T(8,128)S(1)}, f32[64,1024]{1,0:T(8,128)}, u32[]{:S(2)}) copy-start(f32[64,1024]{1,0:T(8,128)} %param.20) | copy-start | bytes 786436
  23.5 94.1 %copy-start.6 = (f32[64,1024]{1,0:T(8,128)S(1)}, f32[64,1024]{1,0:T(8,128)}, u32[]{:S(2)}) copy-start(f32[64,1024]{1,0:T(8,128)} %param.18) | copy-start | bytes 786436
  23.5 94.1 %copy-start.7 = (f32[64,1024]{1,0:T(8,128)S(1)}, f32[64,1024]{1,0:T(8,128)}, u32[]{:S(2)}) copy-start(f32[64,1024]{1,0:T(8,128)} %param.21) | copy-start | bytes 786436
  23.6 94.1 %copy-start.8 = (f32[64,1024]{1,0:T(8,128)S(1)}, f32[64,1024]{1,0:T(8,128)}, u32[]{:S(2)}) copy-start(f32[64,1024]{1,0:T(8,128)} %param.19) | copy-start | bytes 786436
  23.6 94.1 %all-reduce.3.cloned.1.call-start = ((), (), s32[]{:S(2)}) async-start(), calls=%async_computation.2 | async-start | bytes 1048576 | tf_op jit(solution)/shard_map/psum | solution.py:43
  70.1 78.6 %all-gather.4.cloned.1.call-start = ((), (), s32[]{:S(2)}) async-start(), calls=%async_computation.3 | async-start | bytes 1310720 | tf_op jit(solution)/shard_map/all_gather | solution.py:57
  120.5 134.9 %all-gather.6.cloned.1.call-start = ((), (), s32[]{:S(2)}) async-start(), calls=%async_computation.4 | async-start | bytes 5242880 | tf_op jit(solution)/shard_map/all_gather | solution.py:72
  148.7 2.4 copy-start.4
  176.2 160.5 %all-gather.8.cloned.1.call-start = ((), (), s32[]{:S(2)}) async-start(), calls=%async_computation.5 | async-start | bytes 5242880 | tf_op jit(solution)/shard_map/all_gather | solution.py:73
  336.7 4.8 %copy-start.3 = (bf16[2048,1024]{1,0:T(8,128)(2,1)S(1)}, bf16[2048,1024]{1,0:T(8,128)(2,1)}, u32[]{:S(2)}) copy-start(bf16[2048,1024]{1,0:T(8,128)(2,1)} %all-gather.8.cloned.1.call-done) | copy-start | bytes 12582916
Sparse Core Ops, SparseCore 0:
  23.7 46.3 reduce-scatter.1
  73.1 44.5 all-reduce.2
  120.7 27.9 all-gather.3
  176.3 79.0 all-gather.5
  257.5 79.2 all-gather.7
where the time goes:
time: 350 us
  waiting for transfers between devices  277 us (79%)
  matrix products  19.7 us (6%)
  blocking collectives  15.3 us (4%)
  between operations  15.3 us (4%)
  other arithmetic  14.6 us (4%)
  local copies, waits for them, and re-layouts  7.86 us (2%)
    all_gather x1, waiting for transfers between devices, local(): lax.all_gather(gate_new.astype(jnp.bfloat16), 'fs', axis=0, tiled=True)  81.2 us
    all_gather x1, waiting for transfers between devices, local(): lax.all_gather(value_new.astype(jnp.bfloat16), 'fs', axis=0, tiled=True)  73.7 us
    psum x1, waiting for transfers between devices, local(): projected = lax.psum(partial_value, 'rep')  47.5 us
    reduce_scatter x1, waiting for transfers between devices, local(): lax.psum_scatter(jnp.concatenate([value_part, gate_part], axis=1), 'fs',...  46.5 us
    all_gather x1, waiting for transfers between devices, local(): piece = lax.all_gather(scaled, 'fs', axis=0, tiled=True)  28.1 us
    psum x1, blocking collectives, local(): lax.psum((jnp.sum(value_full * value_full), jnp.sum(gate_full * gate_full...  15.3 us
    unnamed x22, local copies, waits for them, and re-layouts  7.86 us
  transfers between devices with their start and end apart: 5, of which 5 were waited for; matrix products, arithmetic and copies ran while one was open for 1% of the time, Pallas kernels for 0%

commit v1 on v0

--- a/solution.py
+++ b/solution.py
@@ -54,7 +54,12 @@
         ],
         axis=1,
     ).astype(jnp.bfloat16)
-    piece = lax.all_gather(scaled, "fs", axis=0, tiled=True)
+    ring = [scaled]
+    for hop in range(3):
+        ring.append(lax.ppermute(ring[-1], "fs", [(dev, (dev + 1) % 4) for dev in range(4)]))
+    piece = jnp.roll(
+        jnp.concatenate(ring[::-1], axis=0), (lax.axis_index("fs") + 1) * ring[0].shape[0], axis=0
+    )
     value_part = jnp.dot(own_value, piece[:, :half_cols], preferred_element_type=jnp.float32)
     gate_part = jnp.dot(own_gate, piece[:, half_cols:], preferred_element_type=jnp.float32)
     expanded = jnp.concatenate([value_part, gate_part], axis=1)

time: 350 us -> 345 us (0.986)
  waiting for transfers between devices: 277 us -> 272 us
    all_gather x1 -> x0, waiting for transfers between devices: 28.1 us -> none  [local(): piece = lax.all_gather(scaled, 'fs', axis=0, tiled=True)]
    ppermute x0 -> x3, waiting for transfers between devices: none -> 24.5 us  [local(): lax.ppermute(ring[-1], 'fs', [(dev, (dev + 1) % 4) for dev in range(4)])]
    unnamed x22 -> x28, local copies, waits for them, and re-layouts: 7.86 us -> 9.03 us
  transfers between devices with their start and end apart: 5 -> 7, of which waited for: 5 -> 7; matrix products, arithmetic and copies ran while one was open for 1% -> 1% of each run, Pallas kernels for 0% -> 0%
where the time goes in v1:
time: 345 us
  waiting for transfers between devices  272 us (79%)
  matrix products  18.4 us (5%)
  between operations  15.3 us (4%)
  blocking collectives  14.2 us (4%)
  other arithmetic  14 us (4%)
  local copies, waits for them, and re-layouts  9.03 us (3%)
    all_gather x1, waiting for transfers between devices, local(): lax.all_gather(gate_new.astype(jnp.bfloat16), 'fs', axis=0, tiled=True)  81.3 us
    all_gather x1, waiting for transfers between devices, local(): lax.all_gather(value_new.astype(jnp.bfloat16), 'fs', axis=0, tiled=True)  72.6 us
    psum x1, waiting for transfers between devices, local(): projected = lax.psum(partial_value, 'rep')  47.5 us
    reduce_scatter x1, waiting for transfers between devices, local(): lax.psum_scatter(jnp.concatenate([value_part, gate_part], axis=1), 'fs',...  46.5 us
    ppermute x3, waiting for transfers between devices, local(): lax.ppermute(ring[-1], 'fs', [(dev, (dev + 1) % 4) for dev in range(4)])  24.5 us
    psum x1, blocking collectives, local(): lax.psum((jnp.sum(value_full * value_full), jnp.sum(gate_full * gate_full...  14.2 us
    unnamed x28, local copies, waits for them, and re-layouts  9.03 us
  transfers between devices with their start and end apart: 7, of which 7 were waited for; matrix products, arithmetic and copies ran while one was open for 1% of the time, Pallas kernels for 0%

profile of v1, /device:TPU:0, one launch (start us, length us, event | category | flops | bytes accessed | tf_op | source)
XLA Modules:
  0.0 345.0 jit_solution(6090410767181007148)
XLA Ops:
  7.2 0.0 copy-start
  7.2 0.0 copy-start.8
  7.2 0.0 reduce-scatter.2.cloned.1.call-start
  7.2 1.2 copy-done
  8.4 0.0 copy-start.9
  8.4 6.0 %fusion.15 = (bf16[2048,256]{1,0:T(8,128)(2,1)S(1)}, f32[2048,256]{1,0:T(8,128)S(1)}) fusion(bf16[2048,2048]{1,0:T(8,128)(2,1)} %param.11, bf16[2048,256]{1,0:T(8,128)(2,1)S(1)} %copy-done), kind=kOutput, calls=%fused_computation.39 | convolution fusion | flops 2148007936 | bytes 12582912 | tf_op jit(solution)/shard_map/dot_general | solution.py:28
  14.4 0.0 copy-done.8
  14.4 0.0 copy-done.9
  14.4 0.0 copy-start.1
  14.4 2.4 fusion.14
  16.9 0.0 copy-done.1
  16.9 1.3 fusion.16
  18.2 0.0 copy-start.2
  18.2 1.3 convolution_add_fusion.1
  19.5 0.9 copy-done.2
  20.4 1.3 fusion.17
  21.6 1.3 convolution_add_fusion
  22.9 1.5 pad_maximum_fusion
  24.4 0.0 reduce-scatter.2.cloned.1.call-update
  24.4 0.0 all-reduce.3.cloned.1.call-start
  24.5 46.5 %reduce-scatter.2.cloned.1.call-done = f32[64,2048]{1,0:T(8,128)} async-done(((f32[256,2048]{1,0:T(8,128)}), f32[64,2048]{1,0:T(8,128)}) %reduce-scatter.2.cloned.1.call-update) | async-done | bytes 524304 | tf_op jit(solution)/shard_map/reduce_scatter | solution.py:40
  70.9 0.0 all-reduce.3.cloned.1.call-update
  71.0 0.0 all-gather.3.cloned.1.call-start
  71.0 47.5 %all-reduce.3.cloned.1.call-done = f32[64,2048]{1,0:T(8,128)} async-done(((f32[64,2048]{1,0:T(8,128)}), f32[64,2048]{1,0:T(8,128)}) %all-reduce.3.cloned.1.call-update) | async-done | bytes 524304 | tf_op jit(solution)/shard_map/psum | solution.py:43
  118.5 0.0 copy-done.4
  118.5 0.0 copy-done.5
  118.5 0.0 copy-done.6
  118.5 0.0 copy-done.7
  118.5 2.1 multiply_convert_fusion.1
  120.7 1.5 collective-permute-start
  122.2 7.8 %collective-permute-done = bf16[64,2048]{1,0:T(8,128)(2,1)S(1)} collective-permute-done((bf16[64,2048]{1,0:T(8,128)(2,1)S(1)}, bf16[64,2048]{1,0:T(8,128)(2,1)S(1)}, u32[]{:S(2)}, u32[]{:S(2)}) %collective-permute-start) | collective-permute-done | bytes 262176 | tf_op jit(solution)/shard_map/ppermute | solution.py:59
  130.0 0.0 collective-permute-start.1
  130.1 8.5 %collective-permute-done.1 = bf16[64,2048]{1,0:T(8,128)(2,1)S(1)} collective-permute-done((bf16[64,2048]{1,0:T(8,128)(2,1)S(1)}, bf16[64,2048]{1,0:T(8,128)(2,1)S(1)}, u32[]{:S(2)}, u32[]{:S(2)}) %collective-permute-start.1) | collective-permute-done | bytes 262176 | tf_op jit(solution)/shard_map/ppermute | solution.py:59
  138.5 0.0 collective-permute-start.2
  138.5 8.2 %collective-permute-done.2 = bf16[64,2048]{1,0:T(8,128)(2,1)S(1)} collective-permute-done((bf16[64,2048]{1,0:T(8,128)(2,1)S(1)}, bf16[64,2048]{1,0:T(8,128)(2,1)S(1)}, u32[]{:S(2)}, u32[]{:S(2)}) %collective-permute-start.2) | collective-permute-done | bytes 262176 | tf_op jit(solution)/shard_map/ppermute | solution.py:59
  146.9 2.6 multiply_reduce_fusion.1
  149.5 2.3 multiply_reduce_fusion
  151.7 14.2 %all-reduce = (f32[]{:T(128)}, f32[]{:T(128)}) all-reduce(f32[]{:T(128)} %get-tuple-element.31, f32[]{:T(128)} %get-tuple-element.33), channel_id=1, replica_groups=mesh['fs'=4,'rep'=4,'tp'=2] {'fs','tp'}, use_global_device_ids=true, to_apply=%region_3.4 | all-reduce | flops 2 | bytes 16 | tf_op jit(solution)/shard_map/psum | solution.py:68
  166.6 5.6 %fusion.11 = (bf16[512,1024]{1,0:T(8,128)(2,1)}, f32[512,1024]{1,0:T(8,128)}, f32[512,1024]{1,0:T(8,128)}) fusion(f32[512,1024]{1,0:T(8,128)} %param.14, f32[512,1024]{1,0:T(8,128)} %get-tuple-element.32, f32[]{:T(128)S(6)} %rsqrt.14), kind=kLoop, calls=%fused_computation.37 | loop fusion | flops 2097152 | bytes 9437188 | tf_op jit(solution)/shard_map/convert_element_type | solution.py:77
  172.2 0.0 all-gather.3.cloned.1.call-update
  172.2 0.0 all-gather.5.cloned.1.call-start
  173.0 4.8 %fusion.10 = (bf16[512,1024]{1,0:T(8,128)(2,1)}, f32[512,1024]{1,0:T(8,128)}, f32[512,1024]{1,0:T(8,128)}) fusion(f32[512,1024]{1,0:T(8,128)} %param.15, f32[512,1024]{1,0:T(8,128)S(1)} %get-tuple-element.34, f32[]{:T(128)S(6)} %rsqrt.15), kind=kLoop, calls=%fused_computation.36 | loop fusion | flops 2097152 | bytes 9437188 | tf_op jit(solution)/shard_map/convert_element_type | solution.py:78
  177.7 0.0 all-gather.5.cloned.1.call-update
  177.7 72.6 %all-gather.3.cloned.1.call-done = bf16[2048,1024]{1,0:T(8,128)(2,1)} async-done(((bf16[512,1024]{1,0:T(8,128)(2,1)}), bf16[2048,1024]{1,0:T(8,128)(2,1)}) %all-gather.3.cloned.1.call-update) | async-done | bytes 4194320 | tf_op jit(solution)/shard_map/all_gather | solution.py:77
  250.3 81.3 %all-gather.5.cloned.1.call-done = bf16[2048,1024]{1,0:T(8,128)(2,1)} async-done(((bf16[512,1024]{1,0:T(8,128)(2,1)}), bf16[2048,1024]{1,0:T(8,128)(2,1)}) %all-gather.5.cloned.1.call-update) | async-done | bytes 4194320 | tf_op jit(solution)/shard_map/all_gather | solution.py:78
  331.6 4.8 %copy.31 = bf16[2048,1024]{1,0:T(8,128)(2,1)} copy(bf16[2048,1024]{1,0:T(8,128)(2,1)} %all-gather.3.cloned.1.call-done) | data formatting | bytes 8388608
  336.4 0.0 copy-done.3
  336.4 2.0 copy.32
  (14 shorter events, 0.2 us)
Async XLA Ops:
  7.2 1.2 copy-start
  7.2 7.2 %copy-start.8 = (bf16[2048,256]{1,0:T(8,128)(2,1)S(1)}, bf16[2048,256]{1,0:T(8,128)(2,1)}, u32[]{:S(2)}) copy-start(bf16[2048,256]{1,0:T(8,128)(2,1)} %param.17) | copy-start | bytes 3145732
  7.2 63.7 %reduce-scatter.2.cloned.1.call-start = ((), (), s32[]{:S(2)}) async-start(), calls=%async_computation.1 | async-start | bytes 2621440 | tf_op jit(solution)/shard_map/reduce_scatter | solution.py:40
  8.4 6.0 %copy-start.9 = (bf16[2048,2048]{1,0:T(8,128)(2,1)S(1)}, bf16[2048,2048]{1,0:T(8,128)(2,1)}, u32[]{:S(2)}) copy-start(bf16[2048,2048]{1,0:T(8,128)(2,1)} %param.11) | copy-start | bytes 25165828
  14.4 2.5 copy-start.1
  18.2 2.2 copy-start.2
  24.4 94.1 %copy-start.4 = (f32[64,1024]{1,0:T(8,128)S(1)}, f32[64,1024]{1,0:T(8,128)}, u32[]{:S(2)}) copy-start(f32[64,1024]{1,0:T(8,128)} %param.20) | copy-start | bytes 786436
  24.4 94.1 %copy-start.5 = (f32[64,1024]{1,0:T(8,128)S(1)}, f32[64,1024]{1,0:T(8,128)}, u32[]{:S(2)}) copy-start(f32[64,1024]{1,0:T(8,128)} %param.18) | copy-start | bytes 786436
  24.4 94.1 %copy-start.6 = (f32[64,1024]{1,0:T(8,128)S(1)}, f32[64,1024]{1,0:T(8,128)}, u32[]{:S(2)}) copy-start(f32[64,1024]{1,0:T(8,128)} %param.21) | copy-start | bytes 786436
  24.4 94.1 %copy-start.7 = (f32[64,1024]{1,0:T(8,128)S(1)}, f32[64,1024]{1,0:T(8,128)}, u32[]{:S(2)}) copy-start(f32[64,1024]{1,0:T(8,128)} %param.19) | copy-start | bytes 786436
  24.4 94.1 %all-reduce.3.cloned.1.call-start = ((), (), s32[]{:S(2)}) async-start(), calls=%async_computation.2 | async-start | bytes 1048576 | tf_op jit(solution)/shard_map/psum | solution.py:43
  71.0 179.4 %all-gather.3.cloned.1.call-start = ((), (), s32[]{:S(2)}) async-start(), calls=%async_computation.3 | async-start | bytes 5242880 | tf_op jit(solution)/shard_map/all_gather | solution.py:77
  120.7 9.4 %collective-permute-start = (bf16[64,2048]{1,0:T(8,128)(2,1)S(1)}, bf16[64,2048]{1,0:T(8,128)(2,1)S(1)}, u32[]{:S(2)}, u32[]{:S(2)}) collective-permute-start(bf16[64,2048]{1,0:T(8,128)(2,1)S(1)} %pad_maximum_fusion.1), channel_id=1, source_target_pairs={{0,8},{8,16},{16,24},{24,0},{1,9},{9,17},{17,25},{25,1},{2,10},{10... | collective-permute-start | bytes 786440 | tf_op jit(solution)/shard_map/ppermute | solution.py:59
  130.0 8.5 %collective-permute-start.1 = (bf16[64,2048]{1,0:T(8,128)(2,1)S(1)}, bf16[64,2048]{1,0:T(8,128)(2,1)S(1)}, u32[]{:S(2)}, u32[]{:S(2)}) collective-permute-start(bf16[64,2048]{1,0:T(8,128)(2,1)S(1)} %collective-permute-done), channel_id=1, source_target_pairs={{0,8},{8,16},{16,24},{24,0},{1,9},{9,17},{17,25},{25,1},{2,10},{10... | collective-permute-start | bytes 786440 | tf_op jit(solution)/shard_map/ppermute | solution.py:59
  138.5 8.2 %collective-permute-start.2 = (bf16[64,2048]{1,0:T(8,128)(2,1)S(1)}, bf16[64,2048]{1,0:T(8,128)(2,1)S(1)}, u32[]{:S(2)}, u32[]{:S(2)}) collective-permute-start(bf16[64,2048]{1,0:T(8,128)(2,1)S(1)} %collective-permute-done.1), channel_id=1, source_target_pairs={{0,8},{8,16},{16,24},{24,0},{1,9},{9,17},{17,25},{25,1},{2,10},{10... | collective-permute-start | bytes 786440 | tf_op jit(solution)/shard_map/ppermute | solution.py:59
  172.2 159.4 %all-gather.5.cloned.1.call-start = ((), (), s32[]{:S(2)}) async-start(), calls=%async_computation.4 | async-start | bytes 5242880 | tf_op jit(solution)/shard_map/all_gather | solution.py:78
  331.6 4.8 %copy-start.3 = (bf16[2048,1024]{1,0:T(8,128)(2,1)S(1)}, bf16[2048,1024]{1,0:T(8,128)(2,1)}, u32[]{:S(2)}) copy-start(bf16[2048,1024]{1,0:T(8,128)(2,1)} %all-gather.5.cloned.1.call-done) | copy-start | bytes 12582916
Sparse Core Ops, SparseCore 0:
  24.5 46.3 reduce-scatter.1
  73.9 44.5 all-reduce.2
  172.3 77.9 all-gather.2
  252.3 79.2 all-gather.4
